TPU v7x, 32 devices: a whole 2x2x4 slice. The times are simulated.
32 devices in a mesh: fs: 4 (over y, x), tp: 8 (over z, core).
Axes of the slice: x: 2, y: 2, z: 4, core: 2. Of those that a mesh axis runs over, the one named last changes fastest.
Arguments:
- tokens: bfloat16 [4096, 2048], P(('fs', 'tp')), may hold values from -6 to 6
- up_gate: bfloat16 [4096, 5632], P('fs', 'tp'), may hold values from -8 to 8
- up_val: bfloat16 [4096, 5632], P('fs', 'tp'), may hold values from -6 to 6
- gate_weight: bfloat16 [2048, 5632], P('fs', 'tp'), may hold values from -0.125 to 0.125
- val_weight: bfloat16 [2048, 5632], P('fs', 'tp'), may hold values from -0.125 to 0.125
- gate_taps: bfloat16 [3, 5632], P(None, 'tp'), may hold values from -3 to 3
- val_taps: bfloat16 [3, 5632], P(None, 'tp'), may hold values from -3 to 3
- hidden_grad: bfloat16 [4096, 5632], P('fs', 'tp'), may hold values from -6 to 6
Outputs:
- input_grad: bfloat16 [4096, 2048], P(('fs', 'tp'))
- gate_weight_grad: float32 [2048, 5632], P('fs', 'tp')
- val_weight_grad: float32 [2048, 5632], P('fs', 'tp')
- gate_taps_grad: float32 [3, 5632], P(None, 'tp')
- val_taps_grad: float32 [3, 5632], P(None, 'tp')
- gate_row_norms: float32 [2048], P('fs')
- val_row_norms: float32 [2048], P('fs')
- tap_row_norms: float32 [2, 3], replicated
All inputs are finite; a program needn't handle non-finite values.
Results may differ from a plain program's by a relative error of at most 0.017.
Values may be sent and summed in bfloat16 or wider, within the bound.
No kernel may reach another device: no remote copies, remote signals or barrier semaphores. Data moves between devices by JAX's collectives and lax.ppermute only.
A program may use at most 128 MiB of HBM per device.

v0:
```python
import jax
import jax.numpy as jnp
from jax import lax
from jax.sharding import PartitionSpec as P

SEQ = 1024


def shifted_sum(padded, kernel, length, backward):
    tap_count = kernel.shape[0]
    result = jnp.zeros((padded.shape[0], length, padded.shape[2]), jnp.float32)
    for tap_index in range(tap_count):
        tap_shift = tap_count - 1 - tap_index if backward else tap_index
        result = (
            result + kernel[tap_index][None, None, :] * padded[:, tap_shift : tap_shift + length]
        )
    return result


def local_grads(up_gate, up_val, hidden_grad, gate_taps, val_taps):
    length = up_gate.shape[1]
    tap_count = gate_taps.shape[0]
    gate_kernel = gate_taps.astype(jnp.float32)
    val_kernel = val_taps.astype(jnp.float32)
    pad_front = ((0, 0), (tap_count - 1, 0), (0, 0))
    pad_back = ((0, 0), (0, tap_count - 1), (0, 0))
    padded_gate = jnp.pad(up_gate.astype(jnp.float32), pad_front)
    padded_val = jnp.pad(up_val.astype(jnp.float32), pad_front)
    conv_gate = shifted_sum(padded_gate, gate_kernel, length, False)
    conv_val = shifted_sum(padded_val, val_kernel, length, False)
    sigmoid_gate = jax.nn.sigmoid(conv_gate)
    grad_hidden = hidden_grad.astype(jnp.float32)
    val_back = grad_hidden * conv_gate * sigmoid_gate
    gate_back = grad_hidden * conv_val * sigmoid_gate * (1.0 + conv_gate * (1.0 - sigmoid_gate))
    up_gate_back = shifted_sum(jnp.pad(gate_back, pad_back), gate_kernel, length, True).astype(
        jnp.bfloat16
    )
    up_val_back = shifted_sum(jnp.pad(val_back, pad_back), val_kernel, length, True).astype(
        jnp.bfloat16
    )
    tap_gate = jnp.stack(
        [
            jnp.sum(padded_gate[:, tap_index : tap_index + length] * gate_back, axis=(0, 1))
            for tap_index in range(tap_count)
        ]
    )
    tap_val = jnp.stack(
        [
            jnp.sum(padded_val[:, tap_index : tap_index + length] * val_back, axis=(0, 1))
            for tap_index in range(tap_count)
        ]
    )
    return (up_gate_back, up_val_back, tap_gate, tap_val)


def local(tokens, up_gate, up_val, gate_weight, val_weight, gate_taps, val_taps, hidden_grad):
    seq_count = up_gate.shape[0] // SEQ

    def as_blocks(values):
        return values.reshape(seq_count, SEQ, values.shape[1])

    gate_back, val_back, tap_gate, tap_val = local_grads(
        as_blocks(up_gate), as_blocks(up_val), as_blocks(hidden_grad), gate_taps, val_taps
    )
    gate_back = gate_back.reshape(up_gate.shape)
    val_back = val_back.reshape(up_val.shape)
    tap_gate, tap_val = lax.psum((tap_gate, tap_val), "fs")
    token_rows = lax.all_gather(tokens, "tp", axis=0, tiled=True)
    weight_contract = (((0,), (0,)), ((), ()))
    joined = jnp.concatenate((gate_back, val_back), axis=1)
    summed = lax.psum_scatter(
        lax.dot_general(
            token_rows, joined, weight_contract, preferred_element_type=jnp.float32
        ).astype(jnp.bfloat16),
        "fs",
        scatter_dimension=0,
        tiled=True,
    ).astype(jnp.float32)
    hidden_block = gate_back.shape[1]
    gate_grad = summed[:, :hidden_block]
    val_grad = summed[:, hidden_block:]
    gate_whole = lax.all_gather(gate_weight, "fs", axis=0, tiled=True)
    val_whole = lax.all_gather(val_weight, "fs", axis=0, tiled=True)
    contract = (((1,), (1,)), ((), ()))
    total = lax.dot_general(gate_back, gate_whole, contract, preferred_element_type=jnp.float32)
    input_grad = lax.psum_scatter(
        (
            total
            + lax.dot_general(val_back, val_whole, contract, preferred_element_type=jnp.float32)
        ).astype(jnp.bfloat16),
        "tp",
        scatter_dimension=0,
        tiled=True,
    )
    tap_squares = jnp.stack(
        [jnp.sum(tap_gate * tap_gate, axis=1), jnp.sum(tap_val * tap_val, axis=1)]
    )
    gate_norms, val_norms, tap_norms = lax.psum(
        (jnp.sum(gate_grad * gate_grad, axis=1), jnp.sum(val_grad * val_grad, axis=1), tap_squares),
        "tp",
    )
    return (input_grad, gate_grad, val_grad, tap_gate, tap_val, gate_norms, val_norms, tap_norms)


def solution(mesh):
    in_specs = (
        P(("fs", "tp"), None),
        P("fs", "tp"),
        P("fs", "tp"),
        P("fs", "tp"),
        P("fs", "tp"),
        P(None, "tp"),
        P(None, "tp"),
        P("fs", "tp"),
    )
    out_specs = (
        P(("fs", "tp"), None),
        P("fs", "tp"),
        P("fs", "tp"),
        P(None, "tp"),
        P(None, "tp"),
        P("fs"),
        P("fs"),
        P(),
    )
    return jax.shard_map(local, mesh=mesh, in_specs=in_specs, out_specs=out_specs, check_vma=False)
```

profile of v0, /device:TPU:0, one launch (start us, length us, event | category | flops | bytes accessed | tf_op | source)
XLA Modules:
  0.0 274.1 jit_solution(9604628618854611853)
XLA Ops:
  7.2 0.7 all-gather.8.cloned.1.call-update
  7.9 0.0 all-gather.4.cloned.1.call-start
  8.0 0.7 all-gather.4.cloned.1.call-update
  8.7 0.7 all-gather.6.cloned.1.call-update
  9.4 0.0 reduce-scatter.5.cloned.1.call-start
  9.5 0.3 convert_bitcast_fusion.1
  9.9 0.4 convert_bitcast_fusion
  10.3 0.2 copy-done.6
  10.6 0.6 copy-done.2
  11.2 10.8 %multiply_reduce_fusion.2 = (f32[704]{0:T(1024)S(1)}, f32[704]{0:T(1024)S(1)}, f32[704]{0:T(1024)S(1)}, f32[1,1024,704]{1,2,0:T(8,128)S(1)}, f32[704]{0:T(1024)S...) fusion(f32[1,1024,704]{1,2,0:T(8,128)S(1)} %convert_bitcast_fusion.1, ...), kind=kLoop, calls=%fused_computation.39 | loop fusion | flops 30994304 | bytes 15893504 | tf_op jit(solution)/shard_map/reduce_sum | solution.py:49
  22.1 4.9 %fusion.21 = (bf16[1024,704]{0,1:T(8,128)(2,1)S(1)}, bf16[1024,704]{0,1:T(8,128)(2,1)S(1)}) fusion(f32[1,1024,704]{1,2,0:T(8,128)S(1)} %get-tuple-element.29, f32[704]{0:T(1024)S(1)} %get-tuple-element.18, f32[704]{0:T(1024)S(1)} %get-tuple-element.19, f32[704]{0:T(1024)S(1)} %get-tuple-element.17, f32[1,1024,704]{1,2,0:T(8,128)S(1)} %get-tuple-element.34, ...), kind=kLoop, calls=%fused_computation.46 | loop fusion | flops 8650752 | bytes 8667648 | tf_op jit(solution)/shard_map/reshape | solution.py:66
  26.9 32.3 %all-gather.8.cloned.1.call-done = bf16[1024,2048]{1,0:T(8,128)(2,1)} async-done(((bf16[128,2048]{1,0:T(8,128)(2,1)}), bf16[1024,2048]{1,0:T(8,128)(2,1)}) %all-gather.8.cloned.1.call-update) | async-done | bytes 4194320 | tf_op jit(solution)/shard_map/all_gather | solution.py:68
  59.2 11.4 %fusion = bf16[2048,1408]{0,1:T(8,128)(2,1)} fusion(bf16[1024,2048]{1,0:T(8,128)(2,1)} %all-gather.8.cloned.1.call-done, bf16[1024,704]{0,1:T(8,128)(2,1)S(1)} %get-tuple-element.37, bf16[1024,704]{0,1:T(8,128)(2,1)S(1)} %get-tuple-element.38), kind=kOutput, calls=%fused_computation.2 | convolution fusion | flops 5914230784 | bytes 12845056 | tf_op jit(solution)/shard_map/dot_general | solution.py:72
  70.6 0.0 reduce-scatter.3.cloned.1.call-start
  70.7 30.7 %all-gather.4.cloned.1.call-done = bf16[2048,704]{0,1:T(8,128)(2,1)} async-done(((bf16[512,704]{0,1:T(8,128)(2,1)}), bf16[2048,704]{0,1:T(8,128)(2,1)}) %all-gather.4.cloned.1.call-update) | async-done | bytes 2883600 | tf_op jit(solution)/shard_map/all_gather | solution.py:82
  101.4 7.5 %fusion.26 = f32[1024,2048]{1,0:T(8,128)} fusion(bf16[1024,704]{0,1:T(8,128)(2,1)S(1)} %get-tuple-element.38, bf16[2048,704]{0,1:T(8,128)(2,1)} %all-gather.4.cloned.1.call-done), kind=kOutput, calls=%fused_computation.60 | convolution fusion | flops 2952790016 | bytes 12713984 | tf_op jit(solution)/shard_map/dot_general | solution.py:85
  108.9 35.9 %all-gather.6.cloned.1.call-done = bf16[2048,704]{0,1:T(8,128)(2,1)} async-done(((bf16[512,704]{0,1:T(8,128)(2,1)}), bf16[2048,704]{0,1:T(8,128)(2,1)}) %all-gather.6.cloned.1.call-update) | async-done | bytes 2883600 | tf_op jit(solution)/shard_map/all_gather | solution.py:83
  144.8 8.2 %add_convert_fusion = bf16[1024,2048]{1,0:T(8,128)(2,1)} fusion(f32[1024,2048]{1,0:T(8,128)} %fusion.26, bf16[1024,704]{0,1:T(8,128)(2,1)S(1)} %get-tuple-element.37, bf16[2048,704]{0,1:T(8,128)(2,1)} %all-gather.6.cloned.1.call-done), kind=kOutput, calls=%fused_computation | convolution fusion | flops 2956984320 | bytes 16908288 | tf_op jit(solution)/shard_map/dot_general | solution.py:89
  153.1 16.9 %all-reduce.5 = (f32[3,704]{1,0:T(4,128)S(1)}, f32[3,704]{1,0:T(4,128)S(1)}) all-reduce(f32[3,704]{1,0:T(4,128)S(1)} %pad_maximum_fusion, f32[3,704]{1,0:T(4,128)S(1)} %pad_maximum_fusion.1), channel_id=1, replica_groups=mesh['fs'=4,'tp'=8] {'fs'}, use_global_device_ids=true, to_apply=%region_5.6 | all-reduce | flops 4224 | bytes 33792 | tf_op jit(solution)/shard_map/psum | solution.py:67
  170.1 0.1 multiply_reduce_fusion.8
  170.2 44.2 %reduce-scatter.5.cloned.1.call-done = bf16[512,1408]{0,1:T(8,128)(2,1)} async-done(((bf16[2048,1408]{0,1:T(8,128)(2,1)}), bf16[512,1408]{0,1:T(8,128)(2,1)}) %reduce-scatter.5.cloned.1.call-update) | async-done | bytes 1441808 | tf_op jit(solution)/shard_map/reduce_scatter | solution.py:71
  214.4 3.3 %multiply_reduce_fusion.6 = (f32[512]{0:T(512)S(1)}, f32[512,704]{0,1:T(8,128)}, f32[512]{0:T(512)S(1)}, f32[512,704]{0,1:T(8,128)}) fusion(bf16[512,1408]{0,1:T(8,128)(2,1)} %reduce-scatter.5.cloned.1.call-done), kind=kLoop, calls=%fused_computation.44 | loop fusion | flops 1440768 | bytes 5771264 | tf_op jit(solution)/shard_map/reduce_sum | solution.py:99
  217.8 17.5 %all-reduce.4 = (f32[512]{0:T(512)}, f32[512]{0:T(512)}, f32[2,3]{1,0:T(2,128)}) all-reduce(f32[512]{0:T(512)S(1)} %get-tuple-element.35, f32[512]{0:T(512)S(1)} %get-tuple-element.25, f32[2,3]{1,0:T(2,128)S(1)} %pad_maximum_fusion.2), channel_id=1, replica_groups=mesh['fs'=4,'tp'=8] {'tp'}, use_global_device_ids=true, to_apply=%region_11.12 | all-reduce | flops 1030 | bytes 8240 | tf_op jit(solution)/shard_map/psum | solution.py:98
  235.2 32.4 %reduce-scatter.3.cloned.1.call-done = bf16[128,2048]{1,0:T(8,128)(2,1)} async-done(((bf16[1024,2048]{1,0:T(8,128)(2,1)}), bf16[128,2048]{1,0:T(8,128)(2,1)}) %reduce-scatter.3.cloned.1.call-update) | async-done | bytes 524304 | tf_op jit(solution)/shard_map/reduce_scatter | solution.py:86
  (29 shorter events, 0.3 us)
Async XLA Ops:
  7.2 2.3 copy-start
  7.2 52.0 %all-gather.8.cloned.1.call-start = ((), (), s32[]{:S(2)}) async-start(), calls=%async_computation.5 | async-start | bytes 4718592 | tf_op jit(solution)/shard_map/all_gather | solution.py:68
  7.9 1.9 copy-start.5
  7.9 2.0 copy-start.1
  7.9 93.5 %all-gather.4.cloned.1.call-start = ((), (), s32[]{:S(2)}) async-start(), calls=%async_computation.2 | async-start | bytes 3604480 | tf_op jit(solution)/shard_map/all_gather | solution.py:82
  8.7 136.2 %all-gather.6.cloned.1.call-start = ((), (), s32[]{:S(2)}) async-start(), calls=%async_computation.3 | async-start | bytes 3604480 | tf_op jit(solution)/shard_map/all_gather | solution.py:83
  9.4 205.0 %reduce-scatter.5.cloned.1.call-start = ((), (), s32[]{:S(2)}) async-start(), calls=%async_computation.6 | async-start | bytes 7208960 | tf_op jit(solution)/shard_map/reduce_scatter | solution.py:71
  9.8 0.7 copy-start.6
  9.8 1.4 copy-start.2
  70.6 197.0 %reduce-scatter.3.cloned.1.call-start = ((), (), s32[]{:S(2)}) async-start(), calls=%async_computation.4 | async-start | bytes 4718592 | tf_op jit(solution)/shard_map/reduce_scatter | solution.py:86
  170.1 47.7 %copy-start.3 = (f32[3,704]{1,0:T(4,128)}, f32[3,704]{1,0:T(4,128)S(1)}, u32[]{:S(2)}) copy-start(f32[3,704]{1,0:T(4,128)S(1)} %get-tuple-element.23) | copy-start | bytes 25348
  170.1 47.7 %copy-start.4 = (f32[3,704]{1,0:T(4,128)}, f32[3,704]{1,0:T(4,128)S(1)}, u32[]{:S(2)}) copy-start(f32[3,704]{1,0:T(4,128)S(1)} %get-tuple-element.24) | copy-start | bytes 25348
Sparse Core Ops, SparseCore 0:
  9.6 49.5 all-gather.7
  61.0 40.3 all-gather.3
  103.3 41.5 all-gather.5
  147.7 66.6 reduce-scatter.4
  217.1 50.4 reduce-scatter.2
where the time goes:
time: 274 us
  waiting for transfers between devices  178 us (65%)
  blocking collectives  34.4 us (13%)
  matrix products  27 us (10%)
  other arithmetic  19.9 us (7%)
  between operations  14 us (5%)
    reduce_scatter x1, waiting for transfers between devices, local(): lax.psum_scatter(lax.dot_general(token_rows, joined, weight_contract, pre...  44.2 us
    all_gather x1, waiting for transfers between devices, local(): val_whole = lax.all_gather(val_weight, 'fs', axis=0, tiled=True)  35.9 us
    reduce_scatter x1, waiting for transfers between devices, local(): lax.psum_scatter((total + lax.dot_general(val_back, val_whole, contract,...  32.4 us
    all_gather x1, waiting for transfers between devices, local(): token_rows = lax.all_gather(tokens, 'tp', axis=0, tiled=True)  32.3 us
    all_gather x1, waiting for transfers between devices, local(): gate_whole = lax.all_gather(gate_weight, 'fs', axis=0, tiled=True)  30.7 us
    psum x1, blocking collectives, local(): lax.psum((jnp.sum(gate_grad * gate_grad, axis=1), jnp.sum(val_grad * val_...  17.5 us
    psum x1, blocking collectives, local(): tap_gate, tap_val = lax.psum((tap_gate, tap_val), 'fs')  16.9 us
    dot_general x1, matrix products, local(): lax.dot_general(token_rows, joined, weight_contract, preferred_element_ty...  11.4 us
  transfers between devices with their start and end apart: 5, of which 5 were waited for; matrix products, arithmetic and copies ran while one was open for 17% of the time, Pallas kernels for 0%

commit v1 on v0

--- a/solution.py
+++ b/solution.py
@@ -79,7 +79,12 @@
     hidden_block = gate_back.shape[1]
     gate_grad = summed[:, :hidden_block]
     val_grad = summed[:, hidden_block:]
-    gate_whole = lax.all_gather(gate_weight, "fs", axis=0, tiled=True)
+    ring = [gate_weight]
+    for hop in range(3):
+        ring.append(lax.ppermute(ring[-1], "fs", [(dev, (dev + 1) % 4) for dev in range(4)]))
+    gate_whole = jnp.roll(
+        jnp.concatenate(ring[::-1], axis=0), (lax.axis_index("fs") + 1) * ring[0].shape[0], axis=0
+    )
     val_whole = lax.all_gather(val_weight, "fs", axis=0, tiled=True)
     contract = (((1,), (1,)), ((), ()))
     total = lax.dot_general(gate_back, gate_whole, contract, preferred_element_type=jnp.float32)

time: 274 us -> 261 us (0.953)
  waiting for transfers between devices: 178 us -> 155 us
  local copies, waits for them, and re-layouts: 1 us -> 9.37 us
  other arithmetic: 19.9 us -> 23 us
    ppermute x0 -> x3, waiting for transfers between devices: none -> 84.1 us  [local(): lax.ppermute(ring[-1], 'fs', [(dev, (dev + 1) % 4) for dev in range(4)])]
    reduce_scatter x1, waiting for transfers between devices: 44.2 us -> 6.77 us  [local(): lax.psum_scatter(lax.dot_general(token_rows, joined, weight_contract, pre...]
    all_gather x1, waiting for transfers between devices: 35.9 us -> 0.01 us  [local(): val_whole = lax.all_gather(val_weight, 'fs', axis=0, tiled=True)]
    all_gather x1 -> x0, waiting for transfers between devices: 30.7 us -> none  [local(): gate_whole = lax.all_gather(gate_weight, 'fs', axis=0, tiled=True)]
    unnamed x14 -> x25, local copies, waits for them, and re-layouts: 0.91 us -> 8.27 us
    reduce_sum x1 -> x2, other arithmetic: 10.8 us -> 11.1 us  [the longest x1 11 us: local_grads(): jnp.sum(padded_gate[:, tap_index:tap_index + length] * gate_back, axis=(0...]
  transfers between devices with their start and end apart: 5 -> 7, of which waited for: 5 -> 6; matrix products, arithmetic and copies ran while one was open for 17% -> 21% of each run, Pallas kernels for 0% -> 0%
where the time goes in v1:
time: 261 us; the launch traced here: 260 us
  waiting for transfers between devices  155 us (59%)
  blocking collectives  33.1 us (13%)
  matrix products  24.4 us (9%)
  other arithmetic  23 us (9%)
  between operations  14 us (5%)
  local copies, waits for them, and re-layouts  9.37 us (4%)
    ppermute x3, waiting for transfers between devices, local(): lax.ppermute(ring[-1], 'fs', [(dev, (dev + 1) % 4) for dev in range(4)])  84.1 us
    reduce_scatter x1, waiting for transfers between devices, local(): lax.psum_scatter((total + lax.dot_general(val_back, val_whole, contract,...  32 us
    all_gather x1, waiting for transfers between devices, local(): token_rows = lax.all_gather(tokens, 'tp', axis=0, tiled=True)  30.6 us
    psum x1, blocking collectives, local(): lax.psum((jnp.sum(gate_grad * gate_grad, axis=1), jnp.sum(val_grad * val_...  17.7 us
    psum x1, blocking collectives, local(): tap_gate, tap_val = lax.psum((tap_gate, tap_val), 'fs')  15.4 us
    dot_general x1, matrix products, local(): lax.dot_general(token_rows, joined, weight_contract, preferred_element_ty...  11.4 us
    reduce_sum x1, other arithmetic, local_grads(): jnp.sum(padded_gate[:, tap_index:tap_index + length] * gate_back, axis=(0...  11 us
    unnamed x25, local copies, waits for them, and re-layouts  8.27 us
  transfers between devices with their start and end apart: 7, of which 6 were waited for; matrix products, arithmetic and copies ran while one was open for 21% of the time, Pallas kernels for 0%

profile of v1, /device:TPU:0, one launch (start us, length us, event | category | flops | bytes accessed | tf_op | source)
XLA Modules:
  0.0 260.3 jit_solution(6819455332922370535)
XLA Ops:
  10.2 2.6 %convert_bitcast_fusion = (f32[1,1024,704]{1,2,0:T(8,128)S(1)}, f32[1,1024,704]{1,2,0:T(8,128)S(1)}) fusion(bf16[1024,704]{0,1:T(8,128)(2,1)} %param.9, bf16[1024,704]{0,1:T(8,128)(2,1)} %param.10), kind=kLoop, calls=%fused_computation.6 | loop fusion | flops 1441792 | bytes 8650752 | tf_op jit(solution)/shard_map/convert_element_type | solution.py:27
  13.3 11.0 %multiply_reduce_fusion.5 = (f32[704]{0:T(1024)S(1)}, f32[704]{0:T(1024)S(1)}, f32[704]{0:T(1024)S(1)}, f32[1,1024,704]{1,2,0:T(8,128)S(1)}, f32[704]{0:T(1024)S...) fusion(f32[1,1024,704]{1,2,0:T(8,128)S(1)} %get-tuple-element.37, ...), kind=kLoop, calls=%fused_computation.42 | loop fusion | flops 30994304 | bytes 15893504 | tf_op jit(solution)/shard_map/reduce_sum | solution.py:43
  24.2 2.2 fusion.23
  26.4 2.2 fusion.22
  28.6 30.6 %all-gather.5.cloned.1.call-done = bf16[1024,2048]{1,0:T(8,128)(2,1)} async-done(((bf16[128,2048]{1,0:T(8,128)(2,1)}), bf16[1024,2048]{1,0:T(8,128)(2,1)}) %all-gather.5.cloned.1.call-update) | async-done | bytes 4194320 | tf_op jit(solution)/shard_map/all_gather | solution.py:68
  59.2 11.4 %fusion = bf16[2048,1408]{0,1:T(8,128)(2,1)} fusion(bf16[1024,2048]{1,0:T(8,128)(2,1)} %all-gather.5.cloned.1.call-done, bf16[1024,704]{0,1:T(8,128)(2,1)S(1)} %fusion.22, bf16[1024,704]{0,1:T(8,128)(2,1)S(1)} %fusion.23), kind=kOutput, calls=%fused_computation.2 | convolution fusion | flops 5914230784 | bytes 12845056 | tf_op jit(solution)/shard_map/dot_general | solution.py:72
  70.7 1.0 copy-done.2
  71.7 1.5 collective-permute-start
  73.2 23.8 %collective-permute-done = bf16[512,704]{0,1:T(8,128)(2,1)S(1)} collective-permute-done((bf16[512,704]{0,1:T(8,128)(2,1)S(1)}, bf16[512,704]{0,1:T(8,128)(2,1)S(1)}, u32[]{:S(2)}, u32[]{:S(2)}) %collective-permute-start) | collective-permute-done | bytes 720928 | tf_op jit(solution)/shard_map/ppermute | solution.py:84
  97.0 28.1 %collective-permute-done.1 = bf16[512,704]{0,1:T(8,128)(2,1)S(1)} collective-permute-done((bf16[512,704]{0,1:T(8,128)(2,1)S(1)}, bf16[512,704]{0,1:T(8,128)(2,1)S(1)}, u32[]{:S(2)}, u32[]{:S(2)}) %collective-permute-start.1) | collective-permute-done | bytes 720928 | tf_op jit(solution)/shard_map/ppermute | solution.py:84
  125.1 32.2 %collective-permute-done.2 = bf16[512,704]{0,1:T(8,128)(2,1)S(1)} collective-permute-done((bf16[512,704]{0,1:T(8,128)(2,1)S(1)}, bf16[512,704]{0,1:T(8,128)(2,1)S(1)}, u32[]{:S(2)}, u32[]{:S(2)}) %collective-permute-start.2) | collective-permute-done | bytes 720928 | tf_op jit(solution)/shard_map/ppermute | solution.py:84
  157.3 1.0 constant_dynamic-update-slice_fusion.7
  158.3 1.0 constant_dynamic-update-slice_fusion.6
  161.1 1.0 constant_dynamic-update-slice_fusion.3
  162.1 1.0 constant_dynamic-update-slice_fusion.2
  163.1 1.0 constant_dynamic-update-slice_fusion.1
  164.1 1.0 constant_dynamic-update-slice_fusion
  165.1 5.9 %fusion.28 = f32[1024,2048]{1,0:T(8,128)S(1)} fusion(bf16[1024,704]{0,1:T(8,128)(2,1)} %copy-done.5, bf16[2048,704]{0,1:T(8,128)(2,1)} %all-gather.3.cloned.1.call-done), kind=kOutput, calls=%fused_computation.70 | convolution fusion | flops 2952790016 | bytes 12713984 | tf_op jit(solution)/shard_map/dot_general | solution.py:94
  171.0 7.2 %add_convert_fusion = bf16[1024,2048]{1,0:T(8,128)(2,1)} fusion(f32[1024,2048]{1,0:T(8,128)S(1)} %fusion.28, bf16[1024,704]{0,1:T(8,128)(2,1)S(1)} %copy-done.4, bf16[4096,704]{0,1:T(8,128)(2,1)} %constant_dynamic-update-slice_fusion, s32[]{:T(128)S(6)} %select_n.14), kind=kOutput, calls=%fused_computation | convolution fusion | flops 2956984320 | bytes 16908292 | tf_op jit(solution)/shard_map/dot_general | solution.py:90
  178.3 15.4 %all-reduce.5 = (f32[3,704]{1,0:T(4,128)S(1)}, f32[3,704]{1,0:T(4,128)S(1)}) all-reduce(f32[3,704]{1,0:T(4,128)S(1)} %pad_maximum_fusion, f32[3,704]{1,0:T(4,128)S(1)} %pad_maximum_fusion.1), channel_id=1, replica_groups=mesh['fs'=4,'tp'=8] {'fs'}, use_global_device_ids=true, to_apply=%region_5.6 | all-reduce | flops 4224 | bytes 33792 | tf_op jit(solution)/shard_map/psum | solution.py:67
  193.9 6.8 %reduce-scatter.5.cloned.1.call-done = bf16[512,1408]{0,1:T(8,128)(2,1)} async-done(((bf16[2048,1408]{0,1:T(8,128)(2,1)}), bf16[512,1408]{0,1:T(8,128)(2,1)}) %reduce-scatter.5.cloned.1.call-update) | async-done | bytes 1441808 | tf_op jit(solution)/shard_map/reduce_scatter | solution.py:71
  200.7 3.3 %multiply_reduce_fusion.6 = (f32[512]{0:T(512)S(1)}, f32[512,704]{0,1:T(8,128)}, f32[512]{0:T(512)S(1)}, f32[512,704]{0,1:T(8,128)}) fusion(bf16[512,1408]{0,1:T(8,128)(2,1)} %reduce-scatter.5.cloned.1.call-done), kind=kLoop, calls=%fused_computation.45 | loop fusion | flops 1440768 | bytes 5771264 | tf_op jit(solution)/shard_map/reduce_sum | solution.py:104
  204.0 17.7 %all-reduce.4 = (f32[512]{0:T(512)}, f32[512]{0:T(512)}, f32[2,3]{1,0:T(2,128)}) all-reduce(f32[512]{0:T(512)S(1)} %get-tuple-element.35, f32[512]{0:T(512)S(1)} %get-tuple-element.25, f32[2,3]{1,0:T(2,128)S(1)} %pad_maximum_fusion.2), channel_id=1, replica_groups=mesh['fs'=4,'tp'=8] {'tp'}, use_global_device_ids=true, to_apply=%region_11.12 | all-reduce | flops 1030 | bytes 8240 | tf_op jit(solution)/shard_map/psum | solution.py:103
  221.8 32.0 %reduce-scatter.3.cloned.1.call-done = bf16[128,2048]{1,0:T(8,128)(2,1)} async-done(((bf16[1024,2048]{1,0:T(8,128)(2,1)}), bf16[128,2048]{1,0:T(8,128)(2,1)}) %reduce-scatter.3.cloned.1.call-update) | async-done | bytes 524304 | tf_op jit(solution)/shard_map/reduce_scatter | solution.py:91
  (44 shorter events, 5.7 us)
Async XLA Ops:
  7.2 52.0 %all-gather.5.cloned.1.call-start = ((), (), s32[]{:S(2)}) async-start(), calls=%async_computation.4 | async-start | bytes 4718592 | tf_op jit(solution)/shard_map/all_gather | solution.py:68
  7.9 157.2 %all-gather.3.cloned.1.call-start = ((), (), s32[]{:S(2)}) async-start(), calls=%async_computation.2 | async-start | bytes 3604480 | tf_op jit(solution)/shard_map/all_gather | solution.py:88
  8.7 192.1 %reduce-scatter.5.cloned.1.call-start = ((), (), s32[]{:S(2)}) async-start(), calls=%async_computation.5 | async-start | bytes 7208960 | tf_op jit(solution)/shard_map/reduce_scatter | solution.py:71
  10.1 2.7 %copy-start = (bf16[1024,704]{0,1:T(8,128)(2,1)S(1)}, bf16[1024,704]{0,1:T(8,128)(2,1)}, u32[]{:S(2)}) copy-start(bf16[1024,704]{0,1:T(8,128)(2,1)} %param.9) | copy-start | bytes 4325380
  10.2 2.7 %copy-start.1 = (bf16[1024,704]{0,1:T(8,128)(2,1)S(1)}, bf16[1024,704]{0,1:T(8,128)(2,1)}, u32[]{:S(2)}) copy-start(bf16[1024,704]{0,1:T(8,128)(2,1)} %param.10) | copy-start | bytes 4325380
  10.2 3.1 %copy-start.6 = (bf16[1024,704]{0,1:T(8,128)(2,1)S(1)}, bf16[1024,704]{0,1:T(8,128)(2,1)}, u32[]{:S(2)}) copy-start(bf16[1024,704]{0,1:T(8,128)(2,1)} %param.15) | copy-start | bytes 4325380
  26.4 44.1 %copy-start.3 = (bf16[1024,704]{0,1:T(8,128)(2,1)}, bf16[1024,704]{0,1:T(8,128)(2,1)S(1)}, u32[]{:S(2)}) copy-start(bf16[1024,704]{0,1:T(8,128)(2,1)S(1)} %fusion.23) | copy-start | bytes 4325380
  28.6 41.9 %copy-start.5 = (bf16[1024,704]{0,1:T(8,128)(2,1)}, bf16[1024,704]{0,1:T(8,128)(2,1)S(1)}, u32[]{:S(2)}) copy-start(bf16[1024,704]{0,1:T(8,128)(2,1)S(1)} %fusion.22) | copy-start | bytes 4325380
  70.6 1.1 copy-start.2
  70.6 183.2 %reduce-scatter.3.cloned.1.call-start = ((), (), s32[]{:S(2)}) async-start(), calls=%async_computation.3 | async-start | bytes 4718592 | tf_op jit(solution)/shard_map/reduce_scatter | solution.py:91
  71.7 25.3 %collective-permute-start = (bf16[512,704]{0,1:T(8,128)(2,1)S(1)}, bf16[512,704]{0,1:T(8,128)(2,1)S(1)}, u32[]{:S(2)}, u32[]{:S(2)}) collective-permute-start(bf16[512,704]{0,1:T(8,128)(2,1)S(1)} %copy-done.2), channel_id=1, source_target_pairs={{0,8},{8,16},{16,24},{24,0},{1,9},{9,17},{17,25},{25,1},{2,10},{10... | collective-permute-start | bytes 2162696 | tf_op jit(solution)/shard_map/ppermute | solution.py:84
  97.0 28.1 %collective-permute-start.1 = (bf16[512,704]{0,1:T(8,128)(2,1)S(1)}, bf16[512,704]{0,1:T(8,128)(2,1)S(1)}, u32[]{:S(2)}, u32[]{:S(2)}) collective-permute-start(bf16[512,704]{0,1:T(8,128)(2,1)S(1)} %collective-permute-done), channel_id=1, source_target_pairs={{0,8},{8,16},{16,24},{24,0},{1,9},{9,17},{17,25},{25,1},{2,10},{10... | collective-permute-start | bytes 2162696 | tf_op jit(solution)/shard_map/ppermute | solution.py:84
  125.1 32.2 %collective-permute-start.2 = (bf16[512,704]{0,1:T(8,128)(2,1)S(1)}, bf16[512,704]{0,1:T(8,128)(2,1)S(1)}, u32[]{:S(2)}, u32[]{:S(2)}) collective-permute-start(bf16[512,704]{0,1:T(8,128)(2,1)S(1)} %collective-permute-done.1), channel_id=1, source_target_pairs={{0,8},{8,16},{16,24},{24,0},{1,9},{9,17},{17,25},{25,1},{2,10},{10... | collective-permute-start | bytes 2162696 | tf_op jit(solution)/shard_map/ppermute | solution.py:84
  165.1 5.9 %copy-start.4 = (bf16[1024,704]{0,1:T(8,128)(2,1)S(1)}, bf16[1024,704]{0,1:T(8,128)(2,1)}, u32[]{:S(2)}) copy-start(bf16[1024,704]{0,1:T(8,128)(2,1)} %copy-done.3) | copy-start | bytes 4325380
  193.7 10.4 %copy-start.7 = (f32[3,704]{1,0:T(4,128)}, f32[3,704]{1,0:T(4,128)S(1)}, u32[]{:S(2)}) copy-start(f32[3,704]{1,0:T(4,128)S(1)} %get-tuple-element.23) | copy-start | bytes 25348
  193.7 10.4 %copy-start.8 = (f32[3,704]{1,0:T(4,128)}, f32[3,704]{1,0:T(4,128)S(1)}, u32[]{:S(2)}) copy-start(f32[3,704]{1,0:T(4,128)S(1)} %get-tuple-element.24) | copy-start | bytes 25348
Sparse Core Ops, SparseCore 0:
  9.6 49.5 all-gather.4
  61.0 57.9 all-gather.2
  122.0 78.6 reduce-scatter.4
  203.4 50.2 reduce-scatter.2
